TPU v7x, 32 devices: a whole 2x2x4 slice. The times are simulated.
32 devices in a mesh: fs: 4 (over y, x), tp: 8 (over z, core).
Axes of the slice: x: 2, y: 2, z: 4, core: 2. Of those that a mesh axis runs over, the one named last changes fastest.
Arguments:
- prompt: bfloat16 [4096, 2048], P(('fs', 'tp')), may hold values from -6 to 6
- norm_gain: float32 [2048], P('tp'), may hold values from 0.1 to 1.9
- gate_master: float32 [8, 2, 512, 2048], P(None, None, 'fs', 'tp'), may hold values from -0.125 to 0.125
- up_master: float32 [8, 2, 512, 2048], P(None, None, 'fs', 'tp'), may hold values from -0.125 to 0.125
- down_master: float32 [8, 2, 512, 2048], P(None, None, 'fs', 'tp'), may hold values from -0.25 to 0.25
- group_pick: int32 [4096, 1], P(('fs', 'tp')), may hold values from 0 to 7; in each aligned block of 128 rows (0 to 127, 128 to 255, ...) at most 32 rows name the same one
- route_weight: bfloat16 [4096, 2], P(('fs', 'tp')), may hold values from 0.099609375 to 1
Outputs:
- gate_serve: bfloat16 [8, 2, 512, 2048], P('tp', None, 'fs')
- up_serve: bfloat16 [8, 2, 512, 2048], P('tp', None, 'fs')
- down_serve: bfloat16 [8, 2, 512, 2048], P('tp', None, 'fs')
- mixed: bfloat16 [4096, 2048], P(('fs', 'tp'))
Inputs may be any that keep to these rules, and one draw needn't show every extreme that they name: `group_pick`: in the rows of one device no group is named by more than 32 rows, and in every draw some device's rows name one group exactly 32 times.
All inputs are finite; a program needn't handle non-finite values.
Results may differ from a plain program's by a relative error of at most 0.0081.
Values may be sent and summed in bfloat16 or wider, within the bound.
A program may use at most 64 MiB of HBM per device.

v0:
```python
import jax
import jax.numpy as jnp
from jax import lax
from jax.sharding import PartitionSpec as P

EPS = 1e-06


def expert_rows(group_rows, weights, pieces):
    gate_piece, up_piece, down_piece = pieces
    expert_count = gate_piece.shape[1]
    unit_count = gate_piece.shape[2]
    model_width = gate_piece.shape[3]
    row_count = group_rows.shape[0]
    gate_matrix = gate_piece.reshape(expert_count * unit_count, model_width)
    up_matrix = up_piece.reshape(expert_count * unit_count, model_width)
    down_matrix = down_piece.reshape(expert_count * unit_count, model_width)
    gate_pre = jnp.einsum("sd,hd->sh", group_rows, gate_matrix, preferred_element_type=jnp.float32)
    up_pre = jnp.einsum("sd,hd->sh", group_rows, up_matrix, preferred_element_type=jnp.float32)
    active = (jax.nn.silu(gate_pre) * up_pre).reshape(row_count, expert_count, unit_count)
    hidden = (weights.astype(jnp.float32)[:, :, None] * active).reshape(
        row_count, expert_count * unit_count
    )
    hidden = hidden.astype(jnp.bfloat16)
    return jnp.dot(hidden, down_matrix, preferred_element_type=jnp.float32)


def per_device(prompt, norm_gain, gate_master, up_master, down_master, group_pick, route_weight):
    group_total = lax.axis_size("tp")
    gate_local = (gate_master * norm_gain).astype(jnp.bfloat16)
    up_local = (up_master * norm_gain).astype(jnp.bfloat16)
    down_local = down_master.astype(jnp.bfloat16)
    gate_serve, up_serve, down_serve = (
        lax.all_to_all(gate_local, "tp", split_axis=0, concat_axis=3, tiled=True),
        lax.all_to_all(up_local, "tp", split_axis=0, concat_axis=3, tiled=True),
        lax.all_to_all(down_local, "tp", split_axis=0, concat_axis=3, tiled=True),
    )
    values = prompt.astype(jnp.float32)
    normed = (values * lax.rsqrt(jnp.mean(values * values, axis=1, keepdims=True) + EPS)).astype(
        jnp.bfloat16
    )
    tok_count = prompt.shape[0]
    capacity = 2 * tok_count // group_total
    slot_total = group_total * capacity
    chosen = group_pick[:, 0]
    member = (chosen[:, None] == jnp.arange(group_total, dtype=jnp.int32)[None, :]).astype(
        jnp.int32
    )
    slot_rank = jnp.sum(jnp.cumsum(member, axis=0) * member, axis=1) - 1
    target = chosen * capacity + slot_rank
    placing = (jnp.arange(slot_total, dtype=jnp.int32)[:, None] == target[None, :]).astype(
        jnp.bfloat16
    )
    send_rows = jnp.dot(placing, normed, preferred_element_type=jnp.float32).astype(jnp.bfloat16)
    send_weights = jnp.dot(placing, route_weight, preferred_element_type=jnp.float32).astype(
        jnp.bfloat16
    )
    got_rows, got_weights = (
        lax.all_to_all(
            send_rows.reshape(group_total, capacity, -1),
            "tp",
            split_axis=0,
            concat_axis=0,
            tiled=True,
        ),
        lax.all_to_all(
            send_weights.reshape(group_total, capacity, -1),
            "tp",
            split_axis=0,
            concat_axis=0,
            tiled=True,
        ),
    )
    group_rows = got_rows.reshape(slot_total, -1)
    weights = got_weights.reshape(slot_total, -1)
    gathered = (
        lax.all_gather(gate_serve, "fs", axis=2, tiled=True),
        lax.all_gather(up_serve, "fs", axis=2, tiled=True),
        lax.all_gather(down_serve, "fs", axis=2, tiled=True),
    )
    summed = expert_rows(group_rows, weights, gathered)
    result = summed.astype(jnp.bfloat16).reshape(group_total, capacity, -1)
    returned = lax.all_to_all(result, "tp", split_axis=0, concat_axis=0, tiled=True)
    mixed = jnp.einsum(
        "st,sd->td", placing, returned.reshape(slot_total, -1), preferred_element_type=jnp.float32
    ).astype(jnp.bfloat16)
    return (gate_serve, up_serve, down_serve, mixed)


def solution(mesh):
    placed = (
        P(("fs", "tp"), None),
        P("tp"),
        P(None, None, "fs", "tp"),
        P(None, None, "fs", "tp"),
        P(None, None, "fs", "tp"),
        P(("fs", "tp"), None),
        P(("fs", "tp"), None),
    )
    return jax.shard_map(
        per_device,
        mesh=mesh,
        in_specs=placed,
        out_specs=(
            P("tp", None, "fs", None),
            P("tp", None, "fs", None),
            P("tp", None, "fs", None),
            P(("fs", "tp"), None),
        ),
        check_vma=False,
    )
```

profile of v0, /device:TPU:0, one launch (start us, length us, event | category | flops | bytes accessed | tf_op | source)
XLA Modules:
  0.0 250.6 jit_solution(5716967491578532564)
XLA Ops:
  7.2 0.0 all-gather.4.cloned.1.call-start
  7.2 2.7 %multiply_convert_fusion = (bf16[8,2,128,256]{3,2,1,0:T(8,128)(2,1)S(1)}, bf16[8,2,128,256]{3,2,1,0:T(8,128)(2,1)S(1)}) fusion(f32[8,2,128,256]{3,2,1,0:T(8,128)} %param.10, f32[256]{0:T(256)} %param.8, f32[8,2,128,256]{3,2,1,0:T(8,128)} %param.9), kind=kLoop, calls=%fused_computation.3 | loop fusion | flops 2097152 | bytes 6292480 | tf_op jit(solution)/shard_map/convert_element_type | solution.py:31
  9.9 32.7 %all_to_all.69 = bf16[8,2,128,256]{3,2,1,0:T(8,128)(2,1)S(1)} all-to-all(bf16[8,2,128,256]{3,2,1,0:T(8,128)(2,1)S(1)} %get-tuple-element.5), channel_id=1, replica_groups=mesh['fs'=4,'tp'=8] {'tp'}, dimensions={0} | all-to-all | bytes 2097152 | tf_op jit(solution)/shard_map/all_to_all | solution.py:34
  42.7 1.1 copy.32
  43.8 0.0 all-gather.6.cloned.1.call-start
  43.8 29.0 %all_to_all.70 = bf16[8,2,128,256]{3,2,1,0:T(8,128)(2,1)S(1)} all-to-all(bf16[8,2,128,256]{3,2,1,0:T(8,128)(2,1)S(1)} %get-tuple-element.4), channel_id=1, replica_groups=mesh['fs'=4,'tp'=8] {'tp'}, dimensions={0} | all-to-all | bytes 2097152 | tf_op jit(solution)/shard_map/all_to_all | solution.py:35
  72.8 1.1 copy.33
  74.0 0.0 all-gather.8.cloned.1.call-start
  74.0 0.1 convert_element_type.46
  74.2 29.0 %all_to_all.71 = bf16[8,2,128,256]{3,2,1,0:T(8,128)(2,1)S(1)} all-to-all(bf16[8,2,128,256]{3,2,1,0:T(8,128)(2,1)S(1)} %convert_element_type.46), channel_id=1, replica_groups=mesh['fs'=4,'tp'=8] {'tp'}, dimensions={0} | all-to-all | bytes 2097152 | tf_op jit(solution)/shard_map/all_to_all | solution.py:36
  103.1 1.1 copy.34
  104.3 0.1 fusion.10
  104.4 0.2 reduce_window_sum.11
  104.5 0.2 select_reduce_fusion
  104.7 0.1 convolution_convert_fusion.3
  104.9 0.1 reshape.61
  105.0 0.6 copy.28
  105.6 3.3 %all-to-all-start.3 = ((bf16[8,32,2]{1,2,0:T(2,128)(2,1)}), bf16[8,32,2]{1,2,0:T(2,128)(2,1)S(1)}, u32[]{:S(2)}, u32[]{:S(2)}) async-start(bf16[8,32,2]{1,2,0:T(2,128)(2,1)} %copy.28), calls=%async_computation.3 | async-start | bytes 8192 | tf_op jit(solution)/shard_map/all_to_all | solution.py:66
  108.9 0.2 fusion.2
  109.1 1.6 convolution_convert_fusion
  110.7 3.7 %all-to-all-done.3 = bf16[8,32,2]{1,2,0:T(2,128)(2,1)S(1)} async-done(((bf16[8,32,2]{1,2,0:T(2,128)(2,1)}), bf16[8,32,2]{1,2,0:T(2,128)(2,1)S(1)}, u32[]{:S(2)}, u32[]{:S(2)}) %all-to-all-start.3) | async-done | bytes 1056 | tf_op jit(solution)/shard_map/all_to_all | solution.py:66
  114.3 3.6 %all-to-all-start.4 = ((bf16[8,32,2048]{2,1,0:T(8,128)(2,1)}), bf16[8,32,2048]{2,1,0:T(8,128)(2,1)S(1)}, u32[]{:S(2)}, u32[]{:S(2)}) async-start(bf16[8,32,2048]{2,1,0:T(8,128)(2,1)} %bitcast.8), calls=%async_computation.4 | async-start | bytes 2097152 | tf_op jit(solution)/shard_map/all_to_all | solution.py:59
  117.9 0.1 copy.31
  118.0 0.3 mul.62
  118.4 0.2 copy.35
  118.6 25.8 %all-to-all-done.4 = bf16[8,32,2048]{2,1,0:T(8,128)(2,1)S(1)} async-done(((bf16[8,32,2048]{2,1,0:T(8,128)(2,1)}), bf16[8,32,2048]{2,1,0:T(8,128)(2,1)S(1)}, u32[]{:S(2)}, u32[]{:S(2)}) %all-to-all-start.4) | async-done | bytes 1048608 | tf_op jit(solution)/shard_map/all_to_all | solution.py:59
  144.4 4.6 %fusion.12 = f32[256,1024]{1,0:T(8,128)} fusion(bf16[256,2048]{1,0:T(8,128)(2,1)S(1)} %bitcast.47, bf16[1024,2048]{1,0:T(8,128)(2,1)} %bitcast.54), kind=kOutput, calls=%fused_computation.26 | convolution fusion | flops 1073741824 | bytes 6291456 | tf_op jit(solution)/shard_map/sd,hd->sh/dot_general | solution.py:18
  149.0 1.4 all-gather.6.cloned.1.call-done
  150.5 55.0 %all-gather.8.cloned.1.call-done = bf16[1,2,512,2048]{3,2,1,0:T(8,128)(2,1)} async-done(((bf16[1,2,128,2048]{3,2,1,0:T(8,128)(2,1)}), bf16[1,2,512,2048]{3,2,1,0:T(8,128)(2,1)}) %all-gather.8.cloned.1.call-update) | async-done | bytes 4194320 | tf_op jit(solution)/shard_map/all_gather | solution.py:79
  205.5 6.4 %convolution_convert_fusion.1 = bf16[256,2048]{1,0:T(8,128)(2,1)S(1)} fusion(bf16[1024,2048]{1,0:T(8,128)(2,1)} %bitcast.56, f32[256,1024]{1,0:T(8,128)S(1)} %bitcast.49, bf16[256,2048]{1,0:T(8,128)(2,1)S(1)} %bitcast.48, bf16[1024,2048]{1,0:T(8,128)(2,1)} %bitcast.55, f32[256,1024]{1,0:T(8,128)} %fusion.12), kind=kOutput, calls=%fused_computation.1 | convolution fusion | flops 2149842944 | bytes 12582912 | tf_op jit(solution)/shard_map/dot_general | solution.py:25
  211.9 31.0 %all_to_all.72 = bf16[8,32,2048]{2,1,0:T(8,128)(2,1)S(1)} all-to-all(bf16[8,32,2048]{2,1,0:T(8,128)(2,1)S(1)} %bitcast.50), channel_id=1, replica_groups=mesh['fs'=4,'tp'=8] {'tp'}, dimensions={0} | all-to-all | bytes 2097152 | tf_op jit(solution)/shard_map/all_to_all | solution.py:83
  242.9 1.1 convolution_convert_fusion.2
  (15 shorter events, 0.1 us)
Async XLA Ops:
  7.2 97.6 %copy-start = (bf16[128,2]{0,1:T(2,128)(2,1)S(1)}, bf16[128,2]{0,1:T(2,128)(2,1)}, u32[]{:S(2)}) copy-start(bf16[128,2]{0,1:T(2,128)(2,1)} %param.13) | copy-start | bytes 1540
  7.2 137.2 %all-gather.4.cloned.1.call-start = ((), (), s32[]{:S(2)}) async-start(), calls=%async_computation.6 | async-start | bytes 5242880 | tf_op jit(solution)/shard_map/all_gather | solution.py:77
  42.7 31.4 %copy-start.1 = (f32[8,2,128,256]{3,2,1,0:T(8,128)S(1)}, f32[8,2,128,256]{3,2,1,0:T(8,128)}, u32[]{:S(2)}) copy-start(f32[8,2,128,256]{3,2,1,0:T(8,128)} %param.11) | copy-start | bytes 6291460
  43.8 106.7 %all-gather.6.cloned.1.call-start = ((), (), s32[]{:S(2)}) async-start(), calls=%async_computation.7 | async-start | bytes 5242880 | tf_op jit(solution)/shard_map/all_gather | solution.py:78
  73.9 30.3 %copy-start.3 = (s32[128,1]{0,1:T(1,128)S(1)}, s32[128,1]{0,1:T(1,128)}, u32[]{:S(2)}) copy-start(s32[128,1]{0,1:T(1,128)} %param.12) | copy-start | bytes 1540
  73.9 35.0 %copy-start.2 = (bf16[128,2048]{1,0:T(8,128)(2,1)S(1)}, bf16[128,2048]{1,0:T(8,128)(2,1)}, u32[]{:S(2)}) copy-start(bf16[128,2048]{1,0:T(8,128)(2,1)} %param.7) | copy-start | bytes 1572868
  74.0 131.5 %all-gather.8.cloned.1.call-start = ((), (), s32[]{:S(2)}) async-start(), calls=%async_computation.8 | async-start | bytes 5242880 | tf_op jit(solution)/shard_map/all_gather | solution.py:79
  105.6 8.8 %all-to-all-start.3 = ((bf16[8,32,2]{1,2,0:T(2,128)(2,1)}), bf16[8,32,2]{1,2,0:T(2,128)(2,1)S(1)}, u32[]{:S(2)}, u32[]{:S(2)}) async-start(bf16[8,32,2]{1,2,0:T(2,128)(2,1)} %copy.28), calls=%async_computation.3 | async-start | bytes 8192 | tf_op jit(solution)/shard_map/all_to_all | solution.py:66
  114.3 30.1 %all-to-all-start.4 = ((bf16[8,32,2048]{2,1,0:T(8,128)(2,1)}), bf16[8,32,2048]{2,1,0:T(8,128)(2,1)S(1)}, u32[]{:S(2)}, u32[]{:S(2)}) async-start(bf16[8,32,2048]{2,1,0:T(8,128)(2,1)} %bitcast.8), calls=%async_computation.4 | async-start | bytes 2097152 | tf_op jit(solution)/shard_map/all_to_all | solution.py:59
Sparse Core Ops, SparseCore 0:
  43.9 51.4 all-gather.3
  97.9 52.5 all-gather.5
  152.9 52.5 all-gather.7
where the time goes:
time: 251 us
  blocking collectives  122 us (49%)
  waiting for transfers between devices  86 us (34%)
  matrix products  13.9 us (6%)
  between operations  13.9 us (6%)
  starting transfers between devices  6.99 us (3%)
  local copies, waits for them, and re-layouts  4.69 us (2%)
  other arithmetic  3.46 us (1%)
    all_gather x1, waiting for transfers between devices, per_device(): lax.all_gather(down_serve, 'fs', axis=2, tiled=True)  55 us
    all_to_all x1, blocking collectives, per_device(): lax.all_to_all(gate_local, 'tp', split_axis=0, concat_axis=3, tiled=True)  32.7 us
    all_to_all x1, blocking collectives, per_device(): lax.all_to_all(result, 'tp', split_axis=0, concat_axis=0, tiled=True)  31 us
    all_to_all x1, blocking collectives, per_device(): lax.all_to_all(up_local, 'tp', split_axis=0, concat_axis=3, tiled=True)  29 us
    all_to_all x1, blocking collectives, per_device(): lax.all_to_all(down_local, 'tp', split_axis=0, concat_axis=3, tiled=True)  29 us
    all_to_all x1, waiting for transfers between devices, per_device(): lax.all_to_all(send_rows.reshape(group_total, capacity, -1), 'tp', split_...  25.8 us
    dot_general x1, matrix products, expert_rows(): return jnp.dot(hidden, down_matrix, preferred_element_type=jnp.float32)  6.42 us
  transfers between devices with their start and end apart: 5, of which 4 were waited for; matrix products, arithmetic and copies ran while one was open for 4% of the time, Pallas kernels for 0%

commit v1 on v0

--- a/solution.py
+++ b/solution.py
@@ -33,7 +33,12 @@
     gate_serve, up_serve, down_serve = (
         lax.all_to_all(gate_local, "tp", split_axis=0, concat_axis=3, tiled=True),
         lax.all_to_all(up_local, "tp", split_axis=0, concat_axis=3, tiled=True),
-        lax.all_to_all(down_local, "tp", split_axis=0, concat_axis=3, tiled=True),
+        jnp.concatenate(
+            lax.all_to_all(
+                jnp.stack(jnp.split(down_local, lax.axis_size("tp"), axis=0)), "tp", 0, 0
+            ),
+            axis=3,
+        ),
     )
     values = prompt.astype(jnp.float32)
     normed = (values * lax.rsqrt(jnp.mean(values * values, axis=1, keepdims=True) + EPS)).astype(

time: 251 us -> 251 us (level)
    all_gather x1, waiting for transfers between devices: 55 us -> 1.31 us  [per_device(): lax.all_gather(down_serve, 'fs', axis=2, tiled=True)]
    all_gather x1, waiting for transfers between devices: 1.44 us -> 55 us  [per_device(): lax.all_gather(up_serve, 'fs', axis=2, tiled=True)]
where the time goes in v1:
time: 251 us
  blocking collectives  122 us (49%)
  waiting for transfers between devices  85.9 us (34%)
  matrix products  13.9 us (6%)
  between operations  13.9 us (6%)
  starting transfers between devices  6.99 us (3%)
  local copies, waits for them, and re-layouts  4.77 us (2%)
  other arithmetic  3.41 us (1%)
    all_gather x1, waiting for transfers between devices, per_device(): lax.all_gather(up_serve, 'fs', axis=2, tiled=True)  55 us
    all_to_all x1, blocking collectives, per_device(): lax.all_to_all(gate_local, 'tp', split_axis=0, concat_axis=3, tiled=True)  32.8 us
    all_to_all x1, blocking collectives, per_device(): lax.all_to_all(result, 'tp', split_axis=0, concat_axis=0, tiled=True)  31 us
    all_to_all x1, blocking collectives, per_device(): lax.all_to_all(jnp.stack(jnp.split(down_local, lax.axis_size('tp'), axis=...  29 us
    all_to_all x1, blocking collectives, per_device(): lax.all_to_all(up_local, 'tp', split_axis=0, concat_axis=3, tiled=True)  29 us
    all_to_all x1, waiting for transfers between devices, per_device(): lax.all_to_all(send_rows.reshape(group_total, capacity, -1), 'tp', split_...  25.8 us
    dot_general x1, matrix products, expert_rows(): return jnp.dot(hidden, down_matrix, preferred_element_type=jnp.float32)  6.43 us
  transfers between devices with their start and end apart: 5, of which 4 were waited for; matrix products, arithmetic and copies ran while one was open for 4% of the time, Pallas kernels for 0%

profile of v1, /device:TPU:0, one launch (start us, length us, event | category | flops | bytes accessed | tf_op | source)
XLA Modules:
  0.0 250.7 jit_solution(1576310928321932488)
XLA Ops:
  7.2 0.0 all-gather.4.cloned.1.call-start
  7.2 2.7 %multiply_convert_fusion = (bf16[8,2,128,256]{3,2,1,0:T(8,128)(2,1)S(1)}, bf16[8,2,128,256]{3,2,1,0:T(8,128)(2,1)S(1)}) fusion(f32[8,2,128,256]{3,2,1,0:T(8,128)} %param.10, f32[256]{0:T(256)} %param.8, f32[8,2,128,256]{3,2,1,0:T(8,128)} %param.9), kind=kLoop, calls=%fused_computation.3 | loop fusion | flops 2097152 | bytes 6292480 | tf_op jit(solution)/shard_map/convert_element_type | solution.py:31
  9.9 32.8 %all_to_all.56 = bf16[8,2,128,256]{3,2,1,0:T(8,128)(2,1)S(1)} all-to-all(bf16[8,2,128,256]{3,2,1,0:T(8,128)(2,1)S(1)} %get-tuple-element.5), channel_id=1, replica_groups=mesh['fs'=4,'tp'=8] {'tp'}, dimensions={0} | all-to-all | bytes 2097152 | tf_op jit(solution)/shard_map/all_to_all | solution.py:34
  42.7 1.1 copy.32
  43.9 0.0 all-gather.8.cloned.1.call-start
  43.9 0.1 convert_element_type.46
  44.2 29.0 %all_to_all.57 = bf16[8,1,2,128,256]{4,3,2,1,0:T(8,128)(2,1)S(1)} all-to-all(bf16[8,1,2,128,256]{4,3,2,1,0:T(8,128)(2,1)S(1)} %fusion.7), channel_id=1, replica_groups=mesh['fs'=4,'tp'=8] {'tp'}, dimensions={0} | all-to-all | bytes 2097152 | tf_op jit(solution)/shard_map/all_to_all | solution.py:37
  73.2 1.1 copy.34
  74.3 0.0 all-gather.6.cloned.1.call-start
  74.4 29.0 %all_to_all.58 = bf16[8,2,128,256]{3,2,1,0:T(8,128)(2,1)S(1)} all-to-all(bf16[8,2,128,256]{3,2,1,0:T(8,128)(2,1)S(1)} %get-tuple-element.4), channel_id=1, replica_groups=mesh['fs'=4,'tp'=8] {'tp'}, dimensions={0} | all-to-all | bytes 2097152 | tf_op jit(solution)/shard_map/all_to_all | solution.py:35
  103.4 1.1 copy.33
  104.5 0.1 fusion.18
  104.6 0.2 reduce_window_sum.11
  104.8 0.2 select_reduce_fusion
  105.0 0.1 convolution_convert_fusion.3
  105.1 0.1 reshape.69
  105.2 0.6 copy.28
  105.8 3.3 %all-to-all-start.3 = ((bf16[8,32,2]{1,2,0:T(2,128)(2,1)}), bf16[8,32,2]{1,2,0:T(2,128)(2,1)S(1)}, u32[]{:S(2)}, u32[]{:S(2)}) async-start(bf16[8,32,2]{1,2,0:T(2,128)(2,1)} %copy.28), calls=%async_computation.3 | async-start | bytes 8192 | tf_op jit(solution)/shard_map/all_to_all | solution.py:71
  109.1 0.2 fusion.2
  109.3 1.6 convolution_convert_fusion
  110.9 3.7 %all-to-all-done.3 = bf16[8,32,2]{1,2,0:T(2,128)(2,1)S(1)} async-done(((bf16[8,32,2]{1,2,0:T(2,128)(2,1)}), bf16[8,32,2]{1,2,0:T(2,128)(2,1)S(1)}, u32[]{:S(2)}, u32[]{:S(2)}) %all-to-all-start.3) | async-done | bytes 1056 | tf_op jit(solution)/shard_map/all_to_all | solution.py:71
  114.6 3.6 %all-to-all-start.4 = ((bf16[8,32,2048]{2,1,0:T(8,128)(2,1)}), bf16[8,32,2048]{2,1,0:T(8,128)(2,1)S(1)}, u32[]{:S(2)}, u32[]{:S(2)}) async-start(bf16[8,32,2048]{2,1,0:T(8,128)(2,1)} %bitcast.15), calls=%async_computation.4 | async-start | bytes 2097152 | tf_op jit(solution)/shard_map/all_to_all | solution.py:64
  118.1 0.1 copy.31
  118.3 0.3 mul.62
  118.6 0.2 copy.35
  118.8 25.8 %all-to-all-done.4 = bf16[8,32,2048]{2,1,0:T(8,128)(2,1)S(1)} async-done(((bf16[8,32,2048]{2,1,0:T(8,128)(2,1)}), bf16[8,32,2048]{2,1,0:T(8,128)(2,1)S(1)}, u32[]{:S(2)}, u32[]{:S(2)}) %all-to-all-start.4) | async-done | bytes 1048608 | tf_op jit(solution)/shard_map/all_to_all | solution.py:64
  144.6 4.6 %fusion.20 = f32[256,1024]{1,0:T(8,128)} fusion(bf16[256,2048]{1,0:T(8,128)(2,1)S(1)} %bitcast.77, bf16[1024,2048]{1,0:T(8,128)(2,1)} %bitcast.84), kind=kOutput, calls=%fused_computation.42 | convolution fusion | flops 1073741824 | bytes 6291456 | tf_op jit(solution)/shard_map/sd,hd->sh/dot_general | solution.py:18
  149.2 1.3 all-gather.8.cloned.1.call-done
  150.6 55.0 %all-gather.6.cloned.1.call-done = bf16[1,2,512,2048]{3,2,1,0:T(8,128)(2,1)} async-done(((bf16[1,2,128,2048]{3,2,1,0:T(8,128)(2,1)}), bf16[1,2,512,2048]{3,2,1,0:T(8,128)(2,1)}) %all-gather.6.cloned.1.call-update) | async-done | bytes 4194320 | tf_op jit(solution)/shard_map/all_gather | solution.py:83
  205.6 6.4 %convolution_convert_fusion.1 = bf16[256,2048]{1,0:T(8,128)(2,1)S(1)} fusion(bf16[1024,2048]{1,0:T(8,128)(2,1)} %bitcast.85, f32[256,1024]{1,0:T(8,128)S(1)} %bitcast.79, bf16[256,2048]{1,0:T(8,128)(2,1)S(1)} %bitcast.78, bf16[1024,2048]{1,0:T(8,128)(2,1)} %bitcast.86, f32[256,1024]{1,0:T(8,128)} %fusion.20), kind=kOutput, calls=%fused_computation.1 | convolution fusion | flops 2149842944 | bytes 12582912 | tf_op jit(solution)/shard_map/dot_general | solution.py:25
  212.0 31.0 %all_to_all.59 = bf16[8,32,2048]{2,1,0:T(8,128)(2,1)S(1)} all-to-all(bf16[8,32,2048]{2,1,0:T(8,128)(2,1)S(1)} %bitcast.80), channel_id=1, replica_groups=mesh['fs'=4,'tp'=8] {'tp'}, dimensions={0} | all-to-all | bytes 2097152 | tf_op jit(solution)/shard_map/all_to_all | solution.py:88
  243.0 1.1 convolution_convert_fusion.2
  (23 shorter events, 0.2 us)
Async XLA Ops:
  7.2 97.8 %copy-start = (bf16[128,2]{0,1:T(2,128)(2,1)S(1)}, bf16[128,2]{0,1:T(2,128)(2,1)}, u32[]{:S(2)}) copy-start(bf16[128,2]{0,1:T(2,128)(2,1)} %param.13) | copy-start | bytes 1540
  7.2 137.4 %all-gather.4.cloned.1.call-start = ((), (), s32[]{:S(2)}) async-start(), calls=%async_computation.6 | async-start | bytes 5242880 | tf_op jit(solution)/shard_map/all_gather | solution.py:82
  9.9 34.0 %copy-start.1 = (f32[8,2,128,256]{3,2,1,0:T(8,128)S(1)}, f32[8,2,128,256]{3,2,1,0:T(8,128)}, u32[]{:S(2)}) copy-start(f32[8,2,128,256]{3,2,1,0:T(8,128)} %param.11) | copy-start | bytes 6291460
  43.9 106.7 %all-gather.8.cloned.1.call-start = ((), (), s32[]{:S(2)}) async-start(), calls=%async_computation.8 | async-start | bytes 5242880 | tf_op jit(solution)/shard_map/all_gather | solution.py:84
  73.2 31.3 %copy-start.3 = (s32[128,1]{0,1:T(1,128)S(1)}, s32[128,1]{0,1:T(1,128)}, u32[]{:S(2)}) copy-start(s32[128,1]{0,1:T(1,128)} %param.12) | copy-start | bytes 1540
  73.2 35.9 %copy-start.2 = (bf16[128,2048]{1,0:T(8,128)(2,1)S(1)}, bf16[128,2048]{1,0:T(8,128)(2,1)}, u32[]{:S(2)}) copy-start(bf16[128,2048]{1,0:T(8,128)(2,1)} %param.7) | copy-start | bytes 1572868
  74.3 131.3 %all-gather.6.cloned.1.call-start = ((), (), s32[]{:S(2)}) async-start(), calls=%async_computation.7 | async-start | bytes 5242880 | tf_op jit(solution)/shard_map/all_gather | solution.py:83
  105.8 8.8 %all-to-all-start.3 = ((bf16[8,32,2]{1,2,0:T(2,128)(2,1)}), bf16[8,32,2]{1,2,0:T(2,128)(2,1)S(1)}, u32[]{:S(2)}, u32[]{:S(2)}) async-start(bf16[8,32,2]{1,2,0:T(2,128)(2,1)} %copy.28), calls=%async_computation.3 | async-start | bytes 8192 | tf_op jit(solution)/shard_map/all_to_all | solution.py:71
  114.6 30.1 %all-to-all-start.4 = ((bf16[8,32,2048]{2,1,0:T(8,128)(2,1)}), bf16[8,32,2048]{2,1,0:T(8,128)(2,1)S(1)}, u32[]{:S(2)}, u32[]{:S(2)}) async-start(bf16[8,32,2048]{2,1,0:T(8,128)(2,1)} %bitcast.15), calls=%async_computation.4 | async-start | bytes 2097152 | tf_op jit(solution)/shard_map/all_to_all | solution.py:64
Sparse Core Ops, SparseCore 0:
  44.0 51.4 all-gather.3
  98.0 52.5 all-gather.7
  153.0 52.5 all-gather.5
